TPU v7x, 256 devices: a 4x2x16 block of a 4x16x16 slice. The times are simulated.
256 devices in a mesh: grp: 2 (over y), ep: 32 (over z, core), tp: 4 (over x).
Axes of the slice: x: 4, y: 2, z: 16, core: 2. Of those that a mesh axis runs over, the one named last changes fastest.
The devices are a block of a 4x16x16 slice.
Arguments:
- outer_gate: bfloat16 [32768, 1024], P(('grp', 'ep'), 'tp'), parts along dimension 0, may hold values from -6 to 6
- inner_gate: bfloat16 [32768, 1024], P(('grp', 'ep'), 'tp'), parts along dimension 0, may hold values from -6 to 6
- conv_input: bfloat16 [32768, 1024], P(('grp', 'ep'), 'tp'), parts along dimension 0, may hold values from -6 to 6
- conv_taps: float32 [3, 1024], P(None, 'tp'), may hold values from -3.5 to 3.5
- mixer_weight: bfloat16 [1024, 2048], P('tp'), may hold values from -0.1875 to 0.1875
- expert_input: bfloat16 [32768, 2048], P(('grp', 'ep', 'tp')), parts along dimension 0, may hold values from -6 to 6
- norm_gain: float32 [2048], replicated, may hold values from 0.1 to 1.9
- expert_ids: int32 [32768, 2], P(('grp', 'ep', 'tp')), parts along dimension 0, may hold values from 0 to 31, all different within a row; in each aligned block of 128 rows (0 to 127, 128 to 255, ...) at most 10 rows name the same one
- route_weight: float32 [32768, 2], P(('grp', 'ep', 'tp')), parts along dimension 0, may hold values from 0.25 to 1
- gate_weight: bfloat16 [32, 2048, 3072], P('ep', None, 'tp'), may hold values from -0.125 to 0.125
- up_weight: bfloat16 [32, 2048, 3072], P('ep', None, 'tp'), may hold values from -0.125 to 0.125
- down_weight: bfloat16 [32, 3072, 2048], P('ep', 'tp'), may hold values from -0.109375 to 0.109375
Outputs:
- mixer_output: bfloat16 [32768, 2048], P(('grp', 'ep', 'tp')), parts along dimension 0
- expert_output: bfloat16 [32768, 2048], P(('grp', 'ep', 'tp')), parts along dimension 0
There are 2 independent parts, one for each index of `grp`. A program takes and returns all parts, laid end to end along the dimension named above; an argument that names none is the same for every part. Nothing has to cross between parts.
Inputs may be any that keep to these rules, and one draw needn't show every extreme that they name: `expert_ids`: each row names 2 different experts. Among the rows of one device no expert is named more than 10 times, a bound that some block reaches.
All inputs are finite; a program needn't handle non-finite values.
Results may differ from a plain program's by a relative error of at most 0.011.
Values may be sent and summed in bfloat16 or wider, within the bound.
A program may use at most 128 MiB of HBM per device.

v0:
```python
import jax
import jax.numpy as jnp
from jax import lax
from jax.sharding import Mesh
from jax.sharding import PartitionSpec as P

TAPS = 3
EP = ("ep_0", "ep_1")
GRP_EP = ("grp", "ep_0", "ep_1")
GRP_EP_TP = ("grp", "ep_0", "ep_1", "tp")
epsilon = 1e-06


def shifted(value, axis, steps):
    count = lax.axis_size(axis)
    initial, last = (max(0, -steps), min(count, count - steps))
    return lax.ppermute(value, axis, [(source, source + steps) for source in range(initial, last)])


def split_up(value, dim, peers):
    lengths = value.shape
    tiles = value.reshape(*lengths[:dim], peers, lengths[dim] // peers, *lengths[dim + 1 :])
    return jnp.moveaxis(tiles, dim, 0)


def summed_on_arrival(value, axis, dim):
    tiles = split_up(value, dim, lax.axis_size(axis))
    arrived = lax.all_to_all(tiles, axis, split_axis=0, concat_axis=0, tiled=True)
    return arrived.astype(jnp.float32).sum(axis=0)


def laid_out(tiles, dim):
    tiles = jnp.moveaxis(tiles, 0, dim)
    lengths = tiles.shape
    return tiles.reshape(*lengths[:dim], lengths[dim] * lengths[dim + 1], *lengths[dim + 2 :])


def exchange_in_order(tiles, axes, order):
    lengths = [lax.axis_size(a) for a in axes]
    tiles = tiles.reshape(*lengths, *tiles.shape[1:])
    for k in order:
        tiles = lax.all_to_all(tiles, axes[k], split_axis=k, concat_axis=k, tiled=True)
    return tiles.reshape(-1, *tiles.shape[len(axes) :])


def two_step_exchange(value, groups, order, split_dim, concat_dim):
    peers = lax.axis_size(groups[0]) * lax.axis_size(groups[1])
    tiles = split_up(value, split_dim, peers)
    return laid_out(exchange_in_order(tiles, groups, order), concat_dim)


def on_device(
    outer_gate,
    inner_gate,
    conv_input,
    conv_taps,
    mixer_weight,
    expert_input,
    norm_gain,
    expert_ids,
    route_weight,
    gate_weight,
    up_weight,
    down_weight,
):
    gated_rows = inner_gate.astype(jnp.float32) * conv_input.astype(jnp.float32)
    length = gated_rows.shape[0]
    earlier = shifted(gated_rows[length - (TAPS - 1) :], EP, 1)
    padded = jnp.concatenate([earlier, gated_rows], axis=0)
    convolved = jnp.zeros_like(gated_rows)
    for tap_index in range(TAPS):
        convolved = convolved + conv_taps[tap_index] * padded[tap_index : tap_index + length]
    mixed = (outer_gate.astype(jnp.float32) * convolved).astype(jnp.bfloat16)
    mixer_output = summed_on_arrival(
        jnp.dot(mixed, mixer_weight, preferred_element_type=jnp.float32).astype(jnp.bfloat16),
        "tp",
        0,
    ).astype(jnp.bfloat16)
    inputs = expert_input.astype(jnp.float32)
    normed = (
        inputs * lax.rsqrt(jnp.mean(inputs * inputs, axis=1, keepdims=True) + epsilon) * norm_gain
    ).astype(jnp.bfloat16)
    tokens_here, top_count = expert_ids.shape
    model_width = expert_input.shape[1]
    expert_count = lax.axis_size(EP) * gate_weight.shape[0]
    capacity = 5 * tokens_here * top_count // (4 * expert_count)
    flat_ids = expert_ids.reshape(-1)
    one_hot = (flat_ids[:, None] == jnp.arange(expert_count, dtype=jnp.int32)[None, :]).astype(
        jnp.int32
    )
    ranks = jnp.sum((jnp.cumsum(one_hot, axis=0) - 1) * one_hot, axis=1)
    target = flat_ids * capacity + ranks
    duplicates = jnp.broadcast_to(
        normed[:, None, :], (tokens_here, top_count, model_width)
    ).reshape(-1, model_width)
    outgoing = (
        jnp.zeros((expert_count * capacity, model_width), jnp.bfloat16).at[target].set(duplicates)
    )
    gate_local = gate_weight[0]
    up_local = up_weight[0]
    down_local = down_weight[0]
    arrived = two_step_exchange(
        outgoing.reshape(expert_count, capacity, model_width), ("ep_0", "ep_1"), (1, 0), 0, 0
    )
    sources = arrived.shape[0]
    slot_count = arrived.shape[1]
    stacked = arrived.reshape(sources * slot_count, model_width)
    block_rows = lax.all_gather(stacked, "tp", axis=0, tiled=True)
    gate_value = jnp.dot(block_rows, gate_local, preferred_element_type=jnp.float32)
    up_value = jnp.dot(block_rows, up_local, preferred_element_type=jnp.float32)
    hidden = (jax.nn.silu(gate_value) * up_value).astype(jnp.bfloat16)
    own_sums = summed_on_arrival(
        jnp.dot(hidden, down_local, preferred_element_type=jnp.float32).astype(jnp.bfloat16),
        "tp",
        0,
    ).astype(jnp.bfloat16)
    answers = two_step_exchange(
        own_sums.reshape(sources, slot_count, model_width), ("ep_0", "ep_1"), (1, 0), 0, 0
    )
    picked = answers.reshape(expert_count * capacity, model_width)[target]
    picked = picked.astype(jnp.float32).reshape(tokens_here, top_count, model_width)
    expert_output = jnp.sum(picked * route_weight[:, :, None], axis=1).astype(jnp.bfloat16)
    return (mixer_output, expert_output)


def solution(mesh):
    finer = Mesh(
        mesh.devices.reshape(mesh.shape["grp"], 16, 2, mesh.shape["tp"]),
        ("grp", "ep_0", "ep_1", "tp"),
    )
    placed = (
        P(GRP_EP, "tp"),
        P(GRP_EP, "tp"),
        P(GRP_EP, "tp"),
        P(None, "tp"),
        P("tp", None),
        P(GRP_EP_TP, None),
        P(),
        P(GRP_EP_TP, None),
        P(GRP_EP_TP, None),
        P(EP, None, "tp"),
        P(EP, None, "tp"),
        P(EP, "tp", None),
    )
    return jax.shard_map(
        on_device,
        mesh=finer,
        in_specs=placed,
        out_specs=(P(GRP_EP_TP, None), P(GRP_EP_TP, None)),
        check_vma=False,
    )
```

profile of v0, /device:TPU:40, one launch (start us, length us, event | category | flops | bytes accessed | tf_op | source)
XLA Modules:
  0.0 410.6 jit_solution(17758050569771702696)
XLA Ops:
  12.7 1.7 broadcast_in_dim.5
  14.4 2.3 reshape.93
  16.8 4.0 scatter_custom_fusion
  20.7 3.3 reshape_reshape_reshape.12
  24.1 2.3 copy.24
  26.4 4.8 %all_to_all.30 = bf16[16,2,1,10,2048]{4,0,3,2,1:T(8,128)(2,1)S(1)} all-to-all(bf16[16,2,1,10,2048]{4,0,3,2,1:T(8,128)(2,1)S(1)} %copy.24), channel_id=1, replica_groups=mesh['grp'=2,'ep_0'=16,'ep_1'=2,'tp'=4] {'ep_1'}, dimensions={1} | all-to-all | bytes 2621440 | tf_op jit(solution)/shard_map/all_to_all | solution.py:42
  31.2 1.3 copy.25
  32.5 87.6 %all_to_all.31 = bf16[16,2,1,10,2048]{4,1,3,2,0:T(2,128)(2,1)S(1)} all-to-all(bf16[16,2,1,10,2048]{4,1,3,2,0:T(2,128)(2,1)S(1)} %copy.25), channel_id=1, replica_groups=mesh['grp'=2,'ep_0'=16,'ep_1'=2,'tp'=4] {'ep_0'}, dimensions={0} | all-to-all | bytes 2621440 | tf_op jit(solution)/shard_map/all_to_all | solution.py:42
  120.1 2.0 copy.26
  122.1 3.6 reshape_reshape_reshape.13
  125.8 58.0 %all-gather.2.cloned.1.call-done = bf16[1280,2048]{1,0:T(8,128)(2,1)} async-done(((bf16[320,2048]{1,0:T(8,128)(2,1)}), bf16[1280,2048]{1,0:T(8,128)(2,1)}) %all-gather.2.cloned.1.call-update) | async-done | bytes 5242896 | tf_op jit(solution)/shard_map/all_gather | solution.py:108
  183.7 7.2 %fusion.3 = f32[1280,768]{1,0:T(8,128)S(1)} fusion(bf16[1280,2048]{1,0:T(8,128)(2,1)} %all-gather.2.cloned.1.call-done, bf16[1,2048,768]{2,1,0:T(8,128)(2,1)} %param.21), kind=kOutput, calls=%fused_computation.7 | convolution fusion | flops 4026531840 | bytes 12320768 | tf_op jit(solution)/shard_map/dot_general | solution.py:109
  191.0 4.8 %fusion = bf16[1280,768]{1,0:T(8,128)(2,1)S(1)} fusion(bf16[1280,2048]{1,0:T(8,128)(2,1)S(1)} %copy-done.8, f32[1280,768]{1,0:T(8,128)S(1)} %fusion.3, bf16[1,2048,768]{2,1,0:T(8,128)(2,1)S(1)} %copy-done.9), kind=kOutput, calls=%fused_computation.4 | convolution fusion | flops 4032430080 | bytes 14286848 | tf_op jit(solution)/shard_map/dot_general | solution.py:110
  195.8 6.1 %convolution_convert_fusion = bf16[1280,2048]{1,0:T(8,128)(2,1)} fusion(bf16[1280,768]{1,0:T(8,128)(2,1)S(1)} %fusion, bf16[1,768,2048]{2,1,0:T(8,128)(2,1)S(1)} %copy-done), kind=kOutput, calls=%fused_computation.2 | convolution fusion | flops 4029153280 | bytes 10354688 | tf_op jit(solution)/shard_map/dot_general | solution.py:113
  201.9 5.3 %all-to-all-start.3 = ((bf16[4,320,2048]{2,1,0:T(8,128)(2,1)}), bf16[4,320,2048]{2,1,0:T(8,128)(2,1)}, u32[]{:S(2)}, u32[]{:S(2)}) async-start(bf16[4,320,2048]{2,1,0:T(8,128)(2,1)} %bitcast.39), calls=%async_computation.3 | async-start | bytes 10485760 | tf_op jit(solution)/shard_map/all_to_all | solution.py:28
  207.3 1.6 collective-permute-start
  209.7 2.1 convolution_convert_fusion.1
  211.8 55.5 %all-to-all-done.3 = bf16[4,320,2048]{2,1,0:T(8,128)(2,1)} async-done(((bf16[4,320,2048]{2,1,0:T(8,128)(2,1)}), bf16[4,320,2048]{2,1,0:T(8,128)(2,1)}, u32[]{:S(2)}, u32[]{:S(2)}) %all-to-all-start.3) | async-done | bytes 5242912 | tf_op jit(solution)/shard_map/all_to_all | solution.py:28
  267.3 5.0 %reduce_sum.57 = bf16[320,2048]{1,0:T(8,128)(2,1)} reduce(bf16[4,320,2048]{2,1,0:T(8,128)(2,1)} %all-to-all-done.3, bf16[]{:T(256)} %constant.9.clone.1), dimensions={0}, to_apply=%region_6.7 | reduce | flops 1966080 | bytes 6553602 | tf_op jit(solution)/shard_map/reduce_sum | solution.py:29
  272.3 2.3 reshape_reshape_reshape.14
  275.4 5.6 %all_to_all.32 = bf16[16,2,1,10,2048]{4,0,3,2,1:T(8,128)(2,1)} all-to-all(bf16[16,2,1,10,2048]{4,0,3,2,1:T(8,128)(2,1)S(1)} %copy.27), channel_id=1, replica_groups=mesh['grp'=2,'ep_0'=16,'ep_1'=2,'tp'=4] {'ep_1'}, dimensions={1} | all-to-all | bytes 2621440 | tf_op jit(solution)/shard_map/all_to_all | solution.py:42
  281.0 3.9 all-to-all-start
  284.9 3.7 copy.28
  288.7 23.1 %all-to-all-done = bf16[4,128,2048]{2,1,0:T(8,128)(2,1)S(1)} async-done(((bf16[4,128,2048]{2,1,0:T(8,128)(2,1)}), bf16[4,128,2048]{2,1,0:T(8,128)(2,1)S(1)}, u32[]{:S(2)}, u32[]{:S(2)}) %all-to-all-start) | async-done | bytes 2097184 | tf_op jit(solution)/shard_map/all_to_all | solution.py:28
  311.8 12.4 %all-to-all-start.5 = ((bf16[16,2,1,10,2048]{4,1,3,2,0:T(2,128)(2,1)}), bf16[16,2,1,10,2048]{4,1,3,2,0:T(2,128)(2,1)}, u32[]{:S(2)}, u32[]{:S(2)}) async-start(bf16[16,2,1,10,2048]{4,1,3,2,0:T(2,128)(2,1)} %copy.28), calls=%async_computation.5 | async-start | bytes 2621440 | tf_op jit(solution)/shard_map/all_to_all | solution.py:42
  324.3 1.3 reduce_sum.53
  325.6 60.9 %all-to-all-done.5 = bf16[16,2,1,10,2048]{4,1,3,2,0:T(2,128)(2,1)} async-done(((bf16[16,2,1,10,2048]{4,1,3,2,0:T(2,128)(2,1)}), bf16[16,2,1,10,2048]{4,1,3,2,0:T(2,128)(2,1)}, u32[]{:S(2)}, u32[]{:S(2)}) %all-to-all-start.5) | async-done | bytes 1310752 | tf_op jit(solution)/shard_map/all_to_all | solution.py:42
  386.5 2.0 copy.29
  388.5 1.3 reshape_reshape_reshape.15
  389.8 5.0 %gather_fusion = bf16[256,2048]{1,0:T(8,128)(2,1)} fusion(bf16[320,2048]{1,0:T(8,128)(2,1)} %reshape_reshape_reshape.15, s32[1024]{0:T(1024)S(1)} %pad_clamp_fusion), kind=kCustom, calls=%fused_computation | custom fusion | bytes 2098176 | tf_op jit(solution)/shard_map/gather | solution.py:120
  394.8 3.4 reshape.80
  398.2 5.6 %multiply_reduce_fusion = bf16[128,2048]{1,0:T(8,128)(2,1)} fusion(f32[128,2,2048]{2,1,0:T(2,128)} %reshape.80, f32[128,2]{1,0:T(8,128)S(1)} %copy.30), kind=kLoop, calls=%fused_computation.10 | loop fusion | flops 786432 | bytes 2622464 | tf_op jit(solution)/shard_map/reduce_sum | solution.py:122
  (45 shorter events, 7.4 us)
Async XLA Ops:
  7.2 188.7 %copy-start = (bf16[1,768,2048]{2,1,0:T(8,128)(2,1)S(1)}, bf16[1,768,2048]{2,1,0:T(8,128)(2,1)}, u32[]{:S(2)}) copy-start(bf16[1,768,2048]{2,1,0:T(8,128)(2,1)} %param.23) | copy-start | bytes 9437188
  7.2 176.5 %all-gather.2.cloned.1.call-start = ((), (), s32[]{:S(2)}) async-start(), calls=%async_computation.6 | async-start | bytes 6553600 | tf_op jit(solution)/shard_map/all_gather | solution.py:108
  183.7 7.3 %copy-start.8 = (bf16[1280,2048]{1,0:T(8,128)(2,1)S(1)}, bf16[1280,2048]{1,0:T(8,128)(2,1)}, u32[]{:S(2)}) copy-start(bf16[1280,2048]{1,0:T(8,128)(2,1)} %all-gather.2.cloned.1.call-done) | copy-start | bytes 15728644
  183.7 7.3 %copy-start.9 = (bf16[1,2048,768]{2,1,0:T(8,128)(2,1)S(1)}, bf16[1,2048,768]{2,1,0:T(8,128)(2,1)}, u32[]{:S(2)}) copy-start(bf16[1,2048,768]{2,1,0:T(8,128)(2,1)} %param.22) | copy-start | bytes 9437188
  201.9 5.3 %copy-start.4 = (bf16[512,256]{1,0:T(8,128)(2,1)S(1)}, bf16[512,256]{1,0:T(8,128)(2,1)}, u32[]{:S(2)}) copy-start(bf16[512,256]{1,0:T(8,128)(2,1)} %param.14) | copy-start | bytes 786436
  201.9 5.3 %copy-start.5 = (bf16[512,256]{1,0:T(8,128)(2,1)S(1)}, bf16[512,256]{1,0:T(8,128)(2,1)}, u32[]{:S(2)}) copy-start(bf16[512,256]{1,0:T(8,128)(2,1)} %param.13) | copy-start | bytes 786436
  201.9 7.0 %copy-start.6 = (f32[3,256]{1,0:T(4,128)S(1)}, f32[3,256]{1,0:T(4,128)}, u32[]{:S(2)}) copy-start(f32[3,256]{1,0:T(4,128)} %param.15) | copy-start | bytes 9220
  201.9 7.8 %copy-start.2 = (bf16[256,2048]{1,0:T(8,128)(2,1)S(1)}, bf16[256,2048]{1,0:T(8,128)(2,1)}, u32[]{:S(2)}) copy-start(bf16[256,2048]{1,0:T(8,128)(2,1)} %param.16) | copy-start | bytes 3145732
  201.9 7.8 %copy-start.3 = (bf16[512,256]{1,0:T(8,128)(2,1)S(1)}, bf16[512,256]{1,0:T(8,128)(2,1)}, u32[]{:S(2)}) copy-start(bf16[512,256]{1,0:T(8,128)(2,1)} %param.12) | copy-start | bytes 786436
  201.9 65.4 %all-to-all-start.3 = ((bf16[4,320,2048]{2,1,0:T(8,128)(2,1)}), bf16[4,320,2048]{2,1,0:T(8,128)(2,1)}, u32[]{:S(2)}, u32[]{:S(2)}) async-start(bf16[4,320,2048]{2,1,0:T(8,128)(2,1)} %bitcast.39), calls=%async_computation.3 | async-start | bytes 10485760 | tf_op jit(solution)/shard_map/all_to_all | solution.py:28
  207.3 2.4 collective-permute-start
  281.0 30.7 %all-to-all-start = ((bf16[4,128,2048]{2,1,0:T(8,128)(2,1)}), bf16[4,128,2048]{2,1,0:T(8,128)(2,1)S(1)}, u32[]{:S(2)}, u32[]{:S(2)}) async-start(bf16[4,128,2048]{2,1,0:T(8,128)(2,1)} %bitcast.3), calls=%async_computation | async-start | bytes 4194304 | tf_op jit(solution)/shard_map/all_to_all | solution.py:28
  284.9 39.2 %copy-start.7 = (f32[128,2]{0,1:T(2,128)S(1)}, f32[128,2]{0,1:T(2,128)}, u32[]{:S(2)}) copy-start(f32[128,2]{0,1:T(2,128)} %param.20) | copy-start | bytes 3076
  311.8 74.7 %all-to-all-start.5 = ((bf16[16,2,1,10,2048]{4,1,3,2,0:T(2,128)(2,1)}), bf16[16,2,1,10,2048]{4,1,3,2,0:T(2,128)(2,1)}, u32[]{:S(2)}, u32[]{:S(2)}) async-start(bf16[16,2,1,10,2048]{4,1,3,2,0:T(2,128)(2,1)} %copy.28), calls=%async_computation.5 | async-start | bytes 2621440 | tf_op jit(solution)/shard_map/all_to_all | solution.py:42
  389.8 14.0 %copy-start.1 = (bf16[1,768,2048]{2,1,0:T(8,128)(2,1)S(1)}, bf16[1,768,2048]{2,1,0:T(8,128)(2,1)}, u32[]{:S(2)}) copy-start(bf16[1,768,2048]{2,1,0:T(8,128)(2,1)} %param.23) | copy-start | bytes 9437188
Sparse Core Ops, SparseCore 0:
  125.9 57.8 all-gather.1
where the time goes:
time: 412 us; the launch traced here: 411 us
  waiting for transfers between devices  198 us (48%)
  blocking collectives  98 us (24%)
  local copies, waits for them, and re-layouts  40.7 us (10%)
  starting transfers between devices  23.2 us (6%)
  matrix products  20.2 us (5%)
  other arithmetic  15.8 us (4%)
  between operations  14.3 us (3%)
    all_to_all x3, blocking collectives, exchange_in_order(): lax.all_to_all(tiles, axes[k], split_axis=k, concat_axis=k, tiled=True)  98 us
    all_to_all x2, waiting for transfers between devices, summed_on_arrival(): lax.all_to_all(tiles, axis, split_axis=0, concat_axis=0, tiled=True)  78.6 us
    all_to_all x1, waiting for transfers between devices, exchange_in_order(): lax.all_to_all(tiles, axes[k], split_axis=k, concat_axis=k, tiled=True)  60.9 us
    all_gather x1, waiting for transfers between devices, on_device(): block_rows = lax.all_gather(stacked, 'tp', axis=0, tiled=True)  58 us
    all_to_all x1, starting transfers between devices, exchange_in_order(): lax.all_to_all(tiles, axes[k], split_axis=k, concat_axis=k, tiled=True)  12.4 us
    all_to_all x2, starting transfers between devices, summed_on_arrival(): lax.all_to_all(tiles, axis, split_axis=0, concat_axis=0, tiled=True)  9.19 us
    all_to_all x4, local copies, waits for them, and re-layouts, exchange_in_order(): lax.all_to_all(tiles, axes[k], split_axis=k, concat_axis=k, tiled=True)  9.04 us
    another operation x4, local copies, waits for them, and re-layouts, exchange_in_order(): tiles = tiles.reshape(*lengths, *tiles.shape[1:])  8.68 us
  transfers between devices with their start and end apart: 5, of which 5 were waited for; matrix products, arithmetic and copies ran while one was open for 2% of the time, Pallas kernels for 0%

commit v1 on v0

--- a/solution.py
+++ b/solution.py
@@ -105,7 +105,9 @@
     sources = arrived.shape[0]
     slot_count = arrived.shape[1]
     stacked = arrived.reshape(sources * slot_count, model_width)
-    block_rows = lax.all_gather(stacked, "tp", axis=0, tiled=True)
+    block_rows = jnp.concatenate(
+        lax.all_to_all(jnp.stack([stacked] * lax.axis_size("tp")), "tp", 0, 0), axis=0
+    )
     gate_value = jnp.dot(block_rows, gate_local, preferred_element_type=jnp.float32)
     up_value = jnp.dot(block_rows, up_local, preferred_element_type=jnp.float32)
     hidden = (jax.nn.silu(gate_value) * up_value).astype(jnp.bfloat16)

time: 412 us -> 396 us (0.961)
  waiting for transfers between devices: 198 us -> 134 us
  blocking collectives: 98 us -> 157 us
  between operations: 14.3 us -> 0.86 us
  starting transfers between devices: 23.2 us -> 27.7 us
    all_to_all x0 -> x1, blocking collectives: none -> 58.9 us  [on_device(): lax.all_to_all(jnp.stack([stacked] * lax.axis_size('tp')), 'tp', 0, 0)]
    all_gather x1 -> x0, waiting for transfers between devices: 58 us -> none  [on_device(): block_rows = lax.all_gather(stacked, 'tp', axis=0, tiled=True)]
    all_to_all x2, waiting for transfers between devices: 78.6 us -> 72.2 us  [summed_on_arrival(): lax.all_to_all(tiles, axis, split_axis=0, concat_axis=0, tiled=True)]
    all_to_all x1, starting transfers between devices: 12.4 us -> 17.2 us  [exchange_in_order(): lax.all_to_all(tiles, axes[k], split_axis=k, concat_axis=k, tiled=True)]
  transfers between devices with their start and end apart: 5 -> 4, of which waited for: 5 -> 4; matrix products, arithmetic and copies ran while one was open for 2% -> 2% of each run, Pallas kernels for 0% -> 0%
where the time goes in v1:
time: 396 us; the launch traced here: 395 us
  blocking collectives  157 us (40%)
  waiting for transfers between devices  134 us (34%)
  local copies, waits for them, and re-layouts  42.8 us (11%)
  starting transfers between devices  27.7 us (7%)
  matrix products  17.3 us (4%)
  other arithmetic  15.8 us (4%)
    all_to_all x3, blocking collectives, exchange_in_order(): lax.all_to_all(tiles, axes[k], split_axis=k, concat_axis=k, tiled=True)  98 us
    all_to_all x2, waiting for transfers between devices, summed_on_arrival(): lax.all_to_all(tiles, axis, split_axis=0, concat_axis=0, tiled=True)  72.2 us
    all_to_all x1, waiting for transfers between devices, exchange_in_order(): lax.all_to_all(tiles, axes[k], split_axis=k, concat_axis=k, tiled=True)  60.9 us
    all_to_all x1, blocking collectives, on_device(): lax.all_to_all(jnp.stack([stacked] * lax.axis_size('tp')), 'tp', 0, 0)  58.9 us
    all_to_all x1, starting transfers between devices, exchange_in_order(): lax.all_to_all(tiles, axes[k], split_axis=k, concat_axis=k, tiled=True)  17.2 us
    all_to_all x4, local copies, waits for them, and re-layouts, exchange_in_order(): lax.all_to_all(tiles, axes[k], split_axis=k, concat_axis=k, tiled=True)  9.04 us
    all_to_all x2, starting transfers between devices, summed_on_arrival(): lax.all_to_all(tiles, axis, split_axis=0, concat_axis=0, tiled=True)  8.97 us
    another operation x4, local copies, waits for them, and re-layouts, exchange_in_order(): tiles = tiles.reshape(*lengths, *tiles.shape[1:])  8.68 us
  transfers between devices with their start and end apart: 4, of which 4 were waited for; matrix products, arithmetic and copies ran while one was open for 2% of the time, Pallas kernels for 0%

profile of v1, /device:TPU:40, one launch (start us, length us, event | category | flops | bytes accessed | tf_op | source)
XLA Modules:
  0.0 395.1 jit_solution(16448142440667117304)
XLA Ops:
  6.1 1.7 broadcast_in_dim.5
  7.8 2.3 reshape.99
  10.1 4.0 %scatter_custom_fusion = bf16[320,2048]{1,0:T(8,128)(2,1)} fusion(s32[256]{0:T(256)S(1)} %bitcast.46, bf16[256,2048]{1,0:T(8,128)(2,1)} %reshape.99, bf16[]{:T(256)} %constant.9.clone.1), kind=kCustom, calls=%fused_computation.16 | custom fusion | bytes 1311232 | tf_op jit(solution)/shard_map/scatter | solution.py:97
  14.1 3.3 reshape_reshape_reshape.9
  17.4 2.3 copy.24
  19.8 4.8 %all_to_all.35 = bf16[16,2,1,10,2048]{4,0,3,2,1:T(8,128)(2,1)S(1)} all-to-all(bf16[16,2,1,10,2048]{4,0,3,2,1:T(8,128)(2,1)S(1)} %copy.24), channel_id=1, replica_groups=mesh['grp'=2,'ep_0'=16,'ep_1'=2,'tp'=4] {'ep_1'}, dimensions={1} | all-to-all | bytes 2621440 | tf_op jit(solution)/shard_map/all_to_all | solution.py:42
  24.6 1.3 copy.25
  25.9 87.6 %all_to_all.36 = bf16[16,2,1,10,2048]{4,1,3,2,0:T(2,128)(2,1)S(1)} all-to-all(bf16[16,2,1,10,2048]{4,1,3,2,0:T(2,128)(2,1)S(1)} %copy.25), channel_id=1, replica_groups=mesh['grp'=2,'ep_0'=16,'ep_1'=2,'tp'=4] {'ep_0'}, dimensions={0} | all-to-all | bytes 2621440 | tf_op jit(solution)/shard_map/all_to_all | solution.py:42
  113.5 2.0 copy.26
  115.5 3.6 stack_reshape_reshape_reshape.2
  119.1 2.0 stack.3
  121.2 58.9 %all_to_all.37 = bf16[4,320,2048]{2,1,0:T(8,128)(2,1)S(1)} all-to-all(bf16[4,320,2048]{2,1,0:T(8,128)(2,1)S(1)} %stack.3), channel_id=1, replica_groups=mesh['grp'=2,'ep_0'=16,'ep_1'=2,'tp'=4] {'tp'}, dimensions={0} | all-to-all | bytes 10485760 | tf_op jit(solution)/shard_map/all_to_all | solution.py:109
  180.1 4.3 %fusion.3 = f32[1280,768]{1,0:T(8,128)S(1)} fusion(bf16[1280,2048]{1,0:T(8,128)(2,1)S(1)} %bitcast.41, bf16[1,2048,768]{2,1,0:T(8,128)(2,1)S(1)} %copy-done.8), kind=kOutput, calls=%fused_computation.7 | convolution fusion | flops 4026531840 | bytes 12320768 | tf_op jit(solution)/shard_map/dot_general | solution.py:111
  184.5 4.8 %fusion = bf16[1280,768]{1,0:T(8,128)(2,1)S(1)} fusion(bf16[1280,2048]{1,0:T(8,128)(2,1)S(1)} %bitcast.42, f32[1280,768]{1,0:T(8,128)S(1)} %fusion.3, bf16[1,2048,768]{2,1,0:T(8,128)(2,1)S(1)} %copy-done.9), kind=kOutput, calls=%fused_computation.4 | convolution fusion | flops 4032430080 | bytes 14286848 | tf_op jit(solution)/shard_map/dot_general | solution.py:112
  189.3 6.1 %convolution_convert_fusion = bf16[1280,2048]{1,0:T(8,128)(2,1)} fusion(bf16[1280,768]{1,0:T(8,128)(2,1)S(1)} %fusion, bf16[1,768,2048]{2,1,0:T(8,128)(2,1)S(1)} %copy-done), kind=kOutput, calls=%fused_computation.2 | convolution fusion | flops 4029153280 | bytes 10354688 | tf_op jit(solution)/shard_map/dot_general | solution.py:115
  195.4 5.3 %all-to-all-start.4 = ((bf16[4,320,2048]{2,1,0:T(8,128)(2,1)}), bf16[4,320,2048]{2,1,0:T(8,128)(2,1)}, u32[]{:S(2)}, u32[]{:S(2)}) async-start(bf16[4,320,2048]{2,1,0:T(8,128)(2,1)} %bitcast.40), calls=%async_computation.4 | async-start | bytes 10485760 | tf_op jit(solution)/shard_map/all_to_all | solution.py:28
  200.7 1.5 collective-permute-start
  202.8 2.1 convolution_convert_fusion.1
  204.9 49.1 %all-to-all-done.4 = bf16[4,320,2048]{2,1,0:T(8,128)(2,1)} async-done(((bf16[4,320,2048]{2,1,0:T(8,128)(2,1)}), bf16[4,320,2048]{2,1,0:T(8,128)(2,1)}, u32[]{:S(2)}, u32[]{:S(2)}) %all-to-all-start.4) | async-done | bytes 5242912 | tf_op jit(solution)/shard_map/all_to_all | solution.py:28
  254.1 5.0 %reduce_sum.57 = bf16[320,2048]{1,0:T(8,128)(2,1)} reduce(bf16[4,320,2048]{2,1,0:T(8,128)(2,1)} %all-to-all-done.4, bf16[]{:T(256)} %constant.9.clone.1), dimensions={0}, to_apply=%region_6.7 | reduce | flops 1966080 | bytes 6553602 | tf_op jit(solution)/shard_map/reduce_sum | solution.py:29
  259.0 2.3 reshape_reshape_reshape.10
  262.1 5.6 %all_to_all.38 = bf16[16,2,1,10,2048]{4,0,3,2,1:T(8,128)(2,1)} all-to-all(bf16[16,2,1,10,2048]{4,0,3,2,1:T(8,128)(2,1)S(1)} %copy.27), channel_id=1, replica_groups=mesh['grp'=2,'ep_0'=16,'ep_1'=2,'tp'=4] {'ep_1'}, dimensions={1} | all-to-all | bytes 2621440 | tf_op jit(solution)/shard_map/all_to_all | solution.py:42
  267.7 3.7 all-to-all-start
  271.4 3.7 copy.28
  275.2 23.1 %all-to-all-done = bf16[4,128,2048]{2,1,0:T(8,128)(2,1)S(1)} async-done(((bf16[4,128,2048]{2,1,0:T(8,128)(2,1)}), bf16[4,128,2048]{2,1,0:T(8,128)(2,1)S(1)}, u32[]{:S(2)}, u32[]{:S(2)}) %all-to-all-start) | async-done | bytes 2097184 | tf_op jit(solution)/shard_map/all_to_all | solution.py:28
  298.2 17.2 %all-to-all-start.6 = ((bf16[16,2,1,10,2048]{4,1,3,2,0:T(2,128)(2,1)}), bf16[16,2,1,10,2048]{4,1,3,2,0:T(2,128)(2,1)}, u32[]{:S(2)}, u32[]{:S(2)}) async-start(bf16[16,2,1,10,2048]{4,1,3,2,0:T(2,128)(2,1)} %copy.28), calls=%async_computation.6 | async-start | bytes 2621440 | tf_op jit(solution)/shard_map/all_to_all | solution.py:42
  316.9 60.9 %all-to-all-done.6 = bf16[16,2,1,10,2048]{4,1,3,2,0:T(2,128)(2,1)} async-done(((bf16[16,2,1,10,2048]{4,1,3,2,0:T(2,128)(2,1)}), bf16[16,2,1,10,2048]{4,1,3,2,0:T(2,128)(2,1)}, u32[]{:S(2)}, u32[]{:S(2)}) %all-to-all-start.6) | async-done | bytes 1310752 | tf_op jit(solution)/shard_map/all_to_all | solution.py:42
  377.8 2.0 copy.29
  379.7 1.3 reshape_reshape_reshape.11
  381.1 5.0 %gather_fusion = bf16[256,2048]{1,0:T(8,128)(2,1)} fusion(bf16[320,2048]{1,0:T(8,128)(2,1)} %reshape_reshape_reshape.11, s32[1024]{0:T(1024)S(1)} %pad_clamp_fusion), kind=kCustom, calls=%fused_computation | custom fusion | bytes 2098176 | tf_op jit(solution)/shard_map/gather | solution.py:122
  386.1 3.4 reshape.86
  389.5 5.6 %multiply_reduce_fusion = bf16[128,2048]{1,0:T(8,128)(2,1)} fusion(f32[128,2,2048]{2,1,0:T(2,128)} %reshape.86, f32[128,2]{1,0:T(8,128)S(1)} %copy.30), kind=kLoop, calls=%fused_computation.10 | loop fusion | flops 786432 | bytes 2622464 | tf_op jit(solution)/shard_map/reduce_sum | solution.py:124
  (44 shorter events, 8.4 us)
Async XLA Ops:
  0.6 188.6 %copy-start = (bf16[1,768,2048]{2,1,0:T(8,128)(2,1)S(1)}, bf16[1,768,2048]{2,1,0:T(8,128)(2,1)}, u32[]{:S(2)}) copy-start(bf16[1,768,2048]{2,1,0:T(8,128)(2,1)} %param.23) | copy-start | bytes 9437188
  121.2 58.9 %copy-start.8 = (bf16[1,2048,768]{2,1,0:T(8,128)(2,1)S(1)}, bf16[1,2048,768]{2,1,0:T(8,128)(2,1)}, u32[]{:S(2)}) copy-start(bf16[1,2048,768]{2,1,0:T(8,128)(2,1)} %param.21) | copy-start | bytes 9437188
  180.1 4.3 %copy-start.9 = (bf16[1,2048,768]{2,1,0:T(8,128)(2,1)S(1)}, bf16[1,2048,768]{2,1,0:T(8,128)(2,1)}, u32[]{:S(2)}) copy-start(bf16[1,2048,768]{2,1,0:T(8,128)(2,1)} %param.22) | copy-start | bytes 9437188
  195.3 5.3 %copy-start.4 = (bf16[512,256]{1,0:T(8,128)(2,1)S(1)}, bf16[512,256]{1,0:T(8,128)(2,1)}, u32[]{:S(2)}) copy-start(bf16[512,256]{1,0:T(8,128)(2,1)} %param.14) | copy-start | bytes 786436
  195.3 5.3 %copy-start.5 = (bf16[512,256]{1,0:T(8,128)(2,1)S(1)}, bf16[512,256]{1,0:T(8,128)(2,1)}, u32[]{:S(2)}) copy-start(bf16[512,256]{1,0:T(8,128)(2,1)} %param.13) | copy-start | bytes 786436
  195.3 6.9 %copy-start.6 = (f32[3,256]{1,0:T(4,128)S(1)}, f32[3,256]{1,0:T(4,128)}, u32[]{:S(2)}) copy-start(f32[3,256]{1,0:T(4,128)} %param.15) | copy-start | bytes 9220
  195.3 7.5 %copy-start.2 = (bf16[256,2048]{1,0:T(8,128)(2,1)S(1)}, bf16[256,2048]{1,0:T(8,128)(2,1)}, u32[]{:S(2)}) copy-start(bf16[256,2048]{1,0:T(8,128)(2,1)} %param.16) | copy-start | bytes 3145732
  195.3 7.5 %copy-start.3 = (bf16[512,256]{1,0:T(8,128)(2,1)S(1)}, bf16[512,256]{1,0:T(8,128)(2,1)}, u32[]{:S(2)}) copy-start(bf16[512,256]{1,0:T(8,128)(2,1)} %param.12) | copy-start | bytes 786436
  195.4 58.7 %all-to-all-start.4 = ((bf16[4,320,2048]{2,1,0:T(8,128)(2,1)}), bf16[4,320,2048]{2,1,0:T(8,128)(2,1)}, u32[]{:S(2)}, u32[]{:S(2)}) async-start(bf16[4,320,2048]{2,1,0:T(8,128)(2,1)} %bitcast.40), calls=%async_computation.4 | async-start | bytes 10485760 | tf_op jit(solution)/shard_map/all_to_all | solution.py:28
  200.7 2.1 collective-permute-start
  267.7 30.5 %all-to-all-start = ((bf16[4,128,2048]{2,1,0:T(8,128)(2,1)}), bf16[4,128,2048]{2,1,0:T(8,128)(2,1)S(1)}, u32[]{:S(2)}, u32[]{:S(2)}) async-start(bf16[4,128,2048]{2,1,0:T(8,128)(2,1)} %bitcast.3), calls=%async_computation | async-start | bytes 4194304 | tf_op jit(solution)/shard_map/all_to_all | solution.py:28
  271.4 44.0 %copy-start.7 = (f32[128,2]{0,1:T(2,128)S(1)}, f32[128,2]{0,1:T(2,128)}, u32[]{:S(2)}) copy-start(f32[128,2]{0,1:T(2,128)} %param.20) | copy-start | bytes 3076
  298.2 79.5 %all-to-all-start.6 = ((bf16[16,2,1,10,2048]{4,1,3,2,0:T(2,128)(2,1)}), bf16[16,2,1,10,2048]{4,1,3,2,0:T(2,128)(2,1)}, u32[]{:S(2)}, u32[]{:S(2)}) async-start(bf16[16,2,1,10,2048]{4,1,3,2,0:T(2,128)(2,1)} %copy.28), calls=%async_computation.6 | async-start | bytes 2621440 | tf_op jit(solution)/shard_map/all_to_all | solution.py:42
  381.1 14.0 %copy-start.1 = (bf16[1,768,2048]{2,1,0:T(8,128)(2,1)S(1)}, bf16[1,768,2048]{2,1,0:T(8,128)(2,1)}, u32[]{:S(2)}) copy-start(bf16[1,768,2048]{2,1,0:T(8,128)(2,1)} %param.23) | copy-start | bytes 9437188
